TPU v7x, 32 devices: a whole 2x2x4 slice. The times are simulated.
32 devices in a mesh: grp: 2 (over y), fs: 4 (over z), tp: 4 (over x, core).
Axes of the slice: x: 2, y: 2, z: 4, core: 2. Of those that a mesh axis runs over, the one named last changes fastest.
Arguments:
- tokens: bfloat16 [2048, 2048], P(('grp', 'fs'), 'tp'), parts along dimension 0, may hold values from -6 to 6
- route_experts: int32 [2048, 2], P(('grp', 'fs')), parts along dimension 0, may hold values from 0 to 15, as said below
- group_weight: float32 [2048], P(('grp', 'fs')), parts along dimension 0, may hold values from 0.2 to 1
- pair_logit: float32 [2048], P(('grp', 'fs')), parts along dimension 0, may hold values from -6 to 6
- norm_gain: float32 [2048], replicated, may hold values from 0.1 to 1.9
- gate_train: float32 [16, 2048, 2048], P(None, 'fs', 'tp'), may hold values from -0.125 to 0.125
- up_train: float32 [16, 2048, 2048], P(None, 'fs', 'tp'), may hold values from -0.125 to 0.125
- down_train: float32 [16, 2048, 2048], P(None, 'fs', 'tp'), may hold values from -0.125 to 0.125
Outputs:
- gate_serve: bfloat16 [32, 2048, 2048], P(('grp', 'fs'), None, 'tp'), parts along dimension 0
- up_serve: bfloat16 [32, 2048, 2048], P(('grp', 'fs'), None, 'tp'), parts along dimension 0
- down_serve: bfloat16 [32, 2048, 2048], P(('grp', 'fs'), None, 'tp'), parts along dimension 0
- moe_out: bfloat16 [2048, 2048], P(('grp', 'fs'), 'tp'), parts along dimension 0
There are 2 independent parts, one for each index of `grp`. A program takes and returns all parts, laid end to end along the dimension named above; an argument that names none is the same for every part. Nothing has to cross between parts.
Inputs may be any that keep to these rules, and one draw needn't show every extreme that they name: `route_experts`: each row names two different experts of the same group of 4 consecutive expert numbers. Among the 256 aligned rows of one index of fs, no expert is named by more than 64 rows, and in every draw some expert is named by exactly 64 rows from every such block.
All inputs are finite; a program needn't handle non-finite values.
Results may differ from a plain program's by a relative error of at most 0.018.
Values may be sent and summed in bfloat16 or wider, within the bound.
No kernel may reach another device: no remote copies, remote signals or barrier semaphores. Data moves between devices by JAX's collectives and lax.ppermute only.
A program may use at most 192 MiB of HBM per device.

v0:
```python
import jax
import jax.numpy as jnp
from jax import lax
from jax.sharding import PartitionSpec as P

CAP = 64


def shards(
    tokens, route_experts, group_weight, pair_logit, norm_gain, gate_train, up_train, down_train
):
    experts = gate_train.shape[0]
    rows_here = gate_train.shape[1]
    model_width = norm_gain.shape[0]
    owners = lax.axis_size("fs")
    per_owner = experts // owners
    tok_rows = tokens.shape[0]
    slots_all = experts * CAP
    start_row = lax.axis_index("fs") * rows_here
    gain_rows = lax.dynamic_slice_in_dim(norm_gain, start_row, rows_here)
    gate_cast = (gain_rows[None, :, None] * gate_train).astype(jnp.bfloat16)
    up_cast = (gain_rows[None, :, None] * up_train).astype(jnp.bfloat16)
    down_cast = down_train.astype(jnp.bfloat16)
    gate_serve, up_serve, down_serve = (
        lax.all_to_all(gate_cast, "fs", split_axis=0, concat_axis=1, tiled=True),
        lax.all_to_all(up_cast, "fs", split_axis=0, concat_axis=1, tiled=True),
        lax.all_to_all(down_cast, "fs", split_axis=0, concat_axis=1, tiled=True),
    )
    expert_ids = jnp.arange(experts, dtype=jnp.int32)
    flat_hits = (route_experts.reshape(tok_rows * 2)[:, None] == expert_ids[None, :]).astype(
        jnp.int32
    )
    before = jnp.cumsum(flat_hits, axis=0) - flat_hits
    slot_index = jnp.sum(before * flat_hits, axis=1) + CAP * route_experts.reshape(tok_rows * 2)
    placed = (slot_index[:, None] == jnp.arange(slots_all, dtype=jnp.int32)[None, :]).reshape(
        tok_rows, 2, slots_all
    )
    pick_rows = (placed[:, 0] | placed[:, 1]).astype(jnp.bfloat16)
    first_gate = group_weight * jax.nn.sigmoid(pair_logit)
    second_gate = group_weight * jax.nn.sigmoid(-pair_logit)
    combine_weights = (
        placed[:, 0].astype(jnp.float32) * first_gate[:, None]
        + placed[:, 1].astype(jnp.float32) * second_gate[:, None]
    )
    contract_rows = (((0,), (0,)), ((), ()))
    outgoing = lax.dot_general(pick_rows, tokens, contract_rows, preferred_element_type=jnp.float32)
    outgoing = outgoing.astype(jnp.bfloat16).reshape(owners, per_owner, CAP, tokens.shape[1])
    arrived = lax.all_to_all(outgoing, "fs", split_axis=0, concat_axis=0, tiled=True)
    section = lax.all_gather(arrived, "tp", axis=3, tiled=True)
    gate_total = jnp.einsum(
        "sexk,ekf->esxf", section, gate_serve, preferred_element_type=jnp.float32
    )
    up_total = jnp.einsum("sexk,ekf->esxf", section, up_serve, preferred_element_type=jnp.float32)
    squares_total = jnp.sum(jnp.square(section.astype(jnp.float32)), axis=3)
    row_scale = jnp.transpose(lax.rsqrt(squares_total / model_width + 1e-06), (1, 0, 2))[..., None]
    hidden = (jax.nn.silu(row_scale * gate_total) * (row_scale * up_total)).astype(jnp.bfloat16)
    summed = lax.psum_scatter(
        jnp.einsum("edf,esxf->dsex", down_serve, hidden, preferred_element_type=jnp.float32).astype(
            jnp.bfloat16
        ),
        "tp",
        scatter_dimension=0,
        tiled=True,
    )
    returned = lax.all_to_all(summed, "fs", split_axis=1, concat_axis=1, tiled=True)
    flat_back = returned.reshape(returned.shape[0], slots_all).astype(jnp.float32)
    moe_out = lax.dot_general(
        combine_weights,
        flat_back,
        (((1,), (1,)), ((), ())),
        precision=lax.Precision.HIGHEST,
        preferred_element_type=jnp.float32,
    )
    return (gate_serve, up_serve, down_serve, moe_out.astype(jnp.bfloat16))


def solution(mesh):
    in_specs = (
        P(("grp", "fs"), "tp"),
        P(("grp", "fs"), None),
        P(("grp", "fs")),
        P(("grp", "fs")),
        P(),
        P(None, "fs", "tp"),
        P(None, "fs", "tp"),
        P(None, "fs", "tp"),
    )
    out_specs = (
        P(("grp", "fs"), None, "tp"),
        P(("grp", "fs"), None, "tp"),
        P(("grp", "fs"), None, "tp"),
        P(("grp", "fs"), "tp"),
    )
    return jax.shard_map(shards, mesh=mesh, in_specs=in_specs, out_specs=out_specs, check_vma=False)
```

profile of v0, /device:TPU:0, one launch (start us, length us, event | category | flops | bytes accessed | tf_op | source)
XLA Modules:
  0.0 724.7 jit_solution(6965078394565885770)
XLA Ops:
  8.3 1.2 reduce-window.6
  11.2 1.5 convolution_convert_fusion
  12.7 6.3 all-to-all-start.3
  19.8 17.1 %multiply_convert_fusion = (bf16[16,512,512]{2,1,0:T(8,128)(2,1)}, bf16[16,512,512]{2,1,0:T(8,128)(2,1)}) fusion(f32[16,512,512]{2,1,0:T(8,128)} %param.14, f32[512]{0:T(512)S(1)} %dynamic_slice.3, f32[16,512,512]{2,1,0:T(8,128)} %param.13), kind=kLoop, calls=%fused_computation | loop fusion | flops 16777216 | bytes 50333696 | tf_op jit(solution)/shard_map/convert_element_type | solution.py:22
  36.9 7.9 %all-to-all-done.3 = bf16[4,4,64,512]{3,2,1,0:T(8,128)(2,1)S(1)} async-done(((bf16[4,4,64,512]{3,2,1,0:T(8,128)(2,1)}), bf16[4,4,64,512]{3,2,1,0:T(8,128)(2,1)S(1)}, u32[]{:S(2)}, u32[]{:S(2)}) %all-to-all-start.3) | async-done | bytes 1048608 | tf_op jit(solution)/shard_map/all_to_all | solution.py:48
  44.8 190.1 %all_to_all.64 = bf16[16,512,512]{2,1,0:T(8,128)(2,1)} all-to-all(bf16[16,512,512]{2,1,0:T(8,128)(2,1)} %get-tuple-element.7), channel_id=1, replica_groups=mesh['grp'=2,'fs'=4,'tp'=4] {'fs'}, dimensions={0} | all-to-all | bytes 16777216 | tf_op jit(solution)/shard_map/all_to_all | solution.py:25
  234.8 5.6 all-to-all-start.1
  240.5 9.0 %convert_element_type.40 = bf16[16,512,512]{2,1,0:T(8,128)(2,1)} convert(f32[16,512,512]{2,1,0:T(8,128)} %param.15) | non-fusion elementwise | flops 4194304 | bytes 25165824 | tf_op jit(solution)/shard_map/convert_element_type | solution.py:23
  249.5 173.1 %all-to-all-done.1 = bf16[16,512,512]{2,1,0:T(8,128)(2,1)} async-done(((bf16[16,512,512]{2,1,0:T(8,128)(2,1)}), bf16[16,512,512]{2,1,0:T(8,128)(2,1)}, u32[]{:S(2)}, u32[]{:S(2)}) %all-to-all-start.1) | async-done | bytes 8388640 | tf_op jit(solution)/shard_map/all_to_all | solution.py:26
  422.6 5.7 all-to-all-start.2
  428.3 1.1 copy.46
  429.6 37.5 %all-gather.2.cloned.1.call-done = bf16[4,4,64,2048]{3,2,0,1:T(8,128)(2,1)} async-done(((bf16[4,4,64,512]{3,2,0,1:T(8,128)(2,1)}), bf16[4,4,64,2048]{3,2,0,1:T(8,128)(2,1)}) %all-gather.2.cloned.1.call-update) | async-done | bytes 4194320 | tf_op jit(solution)/shard_map/all_gather | solution.py:49
  467.1 3.1 multiply_reduce_fusion
  470.2 7.5 %copy.39 = bf16[4,4,512,512]{3,2,0,1:T(8,128)(2,1)} copy(bf16[4,4,512,512]{3,2,1,0:T(8,128)(2,1)} %bitcast.62) | data formatting | bytes 16777216 | tf_op jit(solution)/shard_map/all_to_all | solution.py:25
  477.7 7.5 %copy.40 = bf16[4,4,512,512]{3,2,0,1:T(8,128)(2,1)} copy(bf16[4,4,512,512]{3,2,1,0:T(8,128)(2,1)} %bitcast.3) | data formatting | bytes 16777216 | tf_op jit(solution)/shard_map/all_to_all | solution.py:26
  485.2 125.7 %all-to-all-done.2 = bf16[16,512,512]{2,1,0:T(8,128)(2,1)} async-done(((bf16[16,512,512]{2,1,0:T(8,128)(2,1)}), bf16[16,512,512]{2,1,0:T(8,128)(2,1)}, u32[]{:S(2)}, u32[]{:S(2)}) %all-to-all-start.2) | async-done | bytes 8388640 | tf_op jit(solution)/shard_map/all_to_all | solution.py:27
  610.9 7.7 %copy.41 = bf16[4,4,512,512]{3,2,0,1:T(8,128)(2,1)} copy(bf16[4,4,512,512]{3,2,1,0:T(8,128)(2,1)} %bitcast.6) | data formatting | bytes 16777216 | tf_op jit(solution)/shard_map/all_to_all | solution.py:27
  618.5 7.0 fusion.21
  625.6 14.2 %convert_bitcast_fusion = bf16[2048,4,4,64]{0,3,1,2:T(8,128)(2,1)} fusion(bf16[4,2048,512,1]{2,1,3,0:T(8,128)(2,1)} %bitcast.67, f32[4,4,64,512]{3,2,1,0:T(8,128)} %fusion.21, bf16[4,4,64,2048]{3,2,0,1:T(8,128)(2,1)} %all-gather.2.cloned.1.call-done, bf16[4,2048,512,1]{2,1,3,0:T(8,128)(2,1)} %bitcast.65, f32[4,4,64]{2,1,0:T(4,128)S(1)} %rsqrt_bitcast_fusion), kind=kOutput, calls=%fused_computation.3 | convolution fusion | flops 4301258752 | bytes 27267072 | tf_op jit(solution)/shard_map/edf,esxf->dsex/dot_general | solution.py:58
  639.8 43.7 %reduce-scatter.2.cloned.1.call-done = bf16[512,4,4,64]{0,3,1,2:T(8,128)(2,1)} async-done(((bf16[2048,4,4,64]{0,3,1,2:T(8,128)(2,1)}), bf16[512,4,4,64]{0,3,1,2:T(8,128)(2,1)}) %reduce-scatter.2.cloned.1.call-update) | async-done | bytes 1048592 | tf_op jit(solution)/shard_map/reduce_scatter | solution.py:57
  683.4 2.3 copy.47
  685.7 4.6 all-to-all-start.4
  690.3 25.5 %all-to-all-done.4 = bf16[512,4,4,64]{0,3,2,1:T(8,128)(2,1)S(1)} async-done(((bf16[512,4,4,64]{0,3,2,1:T(8,128)(2,1)}), bf16[512,4,4,64]{0,3,2,1:T(8,128)(2,1)S(1)}, u32[]{:S(2)}, u32[]{:S(2)}) %all-to-all-start.4) | async-done | bytes 1048608 | tf_op jit(solution)/shard_map/all_to_all | solution.py:65
  715.8 2.0 convolution_convert_fusion.1
  (29 shorter events, 3.9 us)
Async XLA Ops:
  7.2 4.0 copy-start
  12.7 32.1 %all-to-all-start.3 = ((bf16[4,4,64,512]{3,2,1,0:T(8,128)(2,1)}), bf16[4,4,64,512]{3,2,1,0:T(8,128)(2,1)S(1)}, u32[]{:S(2)}, u32[]{:S(2)}) async-start(bf16[4,4,64,512]{3,2,1,0:T(8,128)(2,1)} %bitcast.12), calls=%async_computation.3 | async-start | bytes 2097152 | tf_op jit(solution)/shard_map/all_to_all | solution.py:48
  234.8 187.7 %all-to-all-start.1 = ((bf16[16,512,512]{2,1,0:T(8,128)(2,1)}), bf16[16,512,512]{2,1,0:T(8,128)(2,1)}, u32[]{:S(2)}, u32[]{:S(2)}) async-start(bf16[16,512,512]{2,1,0:T(8,128)(2,1)} %get-tuple-element.6), calls=%async_computation.1 | async-start | bytes 16777216 | tf_op jit(solution)/shard_map/all_to_all | solution.py:26
  422.6 188.3 %all-to-all-start.2 = ((bf16[16,512,512]{2,1,0:T(8,128)(2,1)}), bf16[16,512,512]{2,1,0:T(8,128)(2,1)}, u32[]{:S(2)}, u32[]{:S(2)}) async-start(bf16[16,512,512]{2,1,0:T(8,128)(2,1)} %convert_element_type.40), calls=%async_computation.2 | async-start | bytes 16777216 | tf_op jit(solution)/shard_map/all_to_all | solution.py:27
  428.2 38.8 %all-gather.2.cloned.1.call-start = ((), (), s32[]{:S(2)}) async-start(), calls=%async_computation.6 | async-start | bytes 5242880 | tf_op jit(solution)/shard_map/all_gather | solution.py:49
  429.4 254.0 %reduce-scatter.2.cloned.1.call-start = ((), (), s32[]{:S(2)}) async-start(), calls=%async_computation.7 | async-start | bytes 5242880 | tf_op jit(solution)/shard_map/reduce_scatter | solution.py:57
  610.9 7.7 %copy-start.2 = (bf16[4,4,64,2048]{3,2,0,1:T(8,128)(2,1)S(1)}, bf16[4,4,64,2048]{3,2,0,1:T(8,128)(2,1)}, u32[]{:S(2)}) copy-start(bf16[4,4,64,2048]{3,2,0,1:T(8,128)(2,1)} %all-gather.2.cloned.1.call-done) | copy-start | bytes 12582916
  625.6 92.3 %copy-start.1 = (bf16[256,512]{1,0:T(8,128)(2,1)S(1)}, bf16[256,512]{1,0:T(8,128)(2,1)}, u32[]{:S(2)}) copy-start(bf16[256,512]{1,0:T(8,128)(2,1)} %param.8) | copy-start | bytes 786436
  639.7 50.6 %copy-start.3 = (f32[256]{0:T(256)S(1)}, f32[256]{0:T(256)}, u32[]{:S(2)}) copy-start(f32[256]{0:T(256)} %param.10) | copy-start | bytes 3076
  639.7 50.6 %copy-start.4 = (f32[256]{0:T(256)S(1)}, f32[256]{0:T(256)}, u32[]{:S(2)}) copy-start(f32[256]{0:T(256)} %param.11) | copy-start | bytes 3076
  685.7 30.1 %all-to-all-start.4 = ((bf16[512,4,4,64]{0,3,2,1:T(8,128)(2,1)}), bf16[512,4,4,64]{0,3,2,1:T(8,128)(2,1)S(1)}, u32[]{:S(2)}, u32[]{:S(2)}) async-start(bf16[512,4,4,64]{0,3,2,1:T(8,128)(2,1)} %copy.47), calls=%async_computation.5 | async-start | bytes 2097152 | tf_op jit(solution)/shard_map/all_to_all | solution.py:65
Sparse Core Ops, SparseCore 0:
  431.2 35.8 all-gather.1
  639.9 43.4 reduce-scatter.1
where the time goes:
time: 725 us
  waiting for transfers between devices  413 us (57%)
  blocking collectives  190 us (26%)
  other arithmetic  31.5 us (4%)
  local copies, waits for them, and re-layouts  28.4 us (4%)
  matrix products  24.7 us (3%)
  starting transfers between devices  22.5 us (3%)
  between operations  14.1 us (2%)
    all_to_all x1, blocking collectives, shards(): lax.all_to_all(gate_cast, 'fs', split_axis=0, concat_axis=1, tiled=True)  190 us
    all_to_all x1, waiting for transfers between devices, shards(): lax.all_to_all(up_cast, 'fs', split_axis=0, concat_axis=1, tiled=True)  173 us
    all_to_all x1, waiting for transfers between devices, shards(): lax.all_to_all(down_cast, 'fs', split_axis=0, concat_axis=1, tiled=True)  126 us
    reduce_scatter x1, waiting for transfers between devices, shards(): lax.psum_scatter(jnp.einsum('edf,esxf->dsex', down_serve, hidden, preferr...  43.7 us
    all_gather x1, waiting for transfers between devices, shards(): section = lax.all_gather(arrived, 'tp', axis=3, tiled=True)  37.5 us
    all_to_all x1, waiting for transfers between devices, shards(): lax.all_to_all(summed, 'fs', split_axis=1, concat_axis=1, tiled=True)  25.5 us
    convert_element_type x1, other arithmetic, shards(): up_cast = (gain_rows[None, :, None] * up_train).astype(jnp.bfloat16)  17.1 us
  transfers between devices with their start and end apart: 6, of which 6 were waited for; matrix products, arithmetic and copies ran while one was open for 6% of the time, Pallas kernels for 0%

commit v1 on v0

--- a/solution.py
+++ b/solution.py
@@ -4,6 +4,13 @@
 from jax.sharding import PartitionSpec as P
 
 CAP = 64
+
+
+def stacked_exchange(block, axis, split, join):
+    count = lax.axis_size(axis)
+    blocks = jnp.stack(jnp.split(block, count, axis=split), axis=0)
+    blocks = lax.all_to_all(blocks, axis, split_axis=0, concat_axis=0)
+    return jnp.concatenate(blocks, axis=join)
 
 
 def shards(
@@ -22,7 +29,7 @@
     up_cast = (gain_rows[None, :, None] * up_train).astype(jnp.bfloat16)
     down_cast = down_train.astype(jnp.bfloat16)
     gate_serve, up_serve, down_serve = (
-        lax.all_to_all(gate_cast, "fs", split_axis=0, concat_axis=1, tiled=True),
+        stacked_exchange(gate_cast, "fs", 0, 1),
         lax.all_to_all(up_cast, "fs", split_axis=0, concat_axis=1, tiled=True),
         lax.all_to_all(down_cast, "fs", split_axis=0, concat_axis=1, tiled=True),
     )

time: 725 us -> 725 us (level)
    all_to_all x1 -> x0, local copies, waits for them, and re-layouts: 7.52 us -> none  [shards(): lax.all_to_all(gate_cast, 'fs', split_axis=0, concat_axis=1, tiled=True)]
    reshape x0 -> x1, local copies, waits for them, and re-layouts: none -> 7.52 us  [stacked_exchange(): return jnp.concatenate(blocks, axis=join)]
  transfers between devices with their start and end apart: 6 -> 6, of which waited for: 6 -> 6; matrix products, arithmetic and copies ran while one was open for 6% -> 7% of each run, Pallas kernels for 0% -> 0%
where the time goes in v1:
time: 725 us
  waiting for transfers between devices  411 us (57%)
  blocking collectives  190 us (26%)
  other arithmetic  33.3 us (5%)
  local copies, waits for them, and re-layouts  29.4 us (4%)
  matrix products  24.7 us (3%)
  starting transfers between devices  22.5 us (3%)
  between operations  14.1 us (2%)
    all_to_all x1, blocking collectives, stacked_exchange(): blocks = lax.all_to_all(blocks, axis, split_axis=0, concat_axis=0)  190 us
    all_to_all x1, waiting for transfers between devices, shards(): lax.all_to_all(up_cast, 'fs', split_axis=0, concat_axis=1, tiled=True)  173 us
    all_to_all x1, waiting for transfers between devices, shards(): lax.all_to_all(down_cast, 'fs', split_axis=0, concat_axis=1, tiled=True)  126 us
    reduce_scatter x1, waiting for transfers between devices, shards(): lax.psum_scatter(jnp.einsum('edf,esxf->dsex', down_serve, hidden, preferr...  43.7 us
    all_gather x1, waiting for transfers between devices, shards(): section = lax.all_gather(arrived, 'tp', axis=3, tiled=True)  37.5 us
    all_to_all x1, waiting for transfers between devices, shards(): lax.all_to_all(summed, 'fs', split_axis=1, concat_axis=1, tiled=True)  25.5 us
    convert_element_type x1, other arithmetic, shards(): up_cast = (gain_rows[None, :, None] * up_train).astype(jnp.bfloat16)  15 us
  transfers between devices with their start and end apart: 6, of which 6 were waited for; matrix products, arithmetic and copies ran while one was open for 7% of the time, Pallas kernels for 0%

profile of v1, /device:TPU:0, one launch (start us, length us, event | category | flops | bytes accessed | tf_op | source)
XLA Modules:
  0.0 724.7 jit_solution(15451589766170905185)
XLA Ops:
  8.3 1.2 reduce-window.6
  11.2 1.5 convolution_convert_fusion
  12.7 6.3 all-to-all-start.3
  19.8 15.0 %multiply_convert_fusion = (bf16[16,512,512]{2,1,0:T(8,128)(2,1)}, bf16[16,512,512]{2,1,0:T(8,128)(2,1)S(1)}) fusion(f32[16,512,512]{2,1,0:T(8,128)} %param.14, f32[512]{0:T(512)S(1)} %dynamic_slice.3, f32[16,512,512]{2,1,0:T(8,128)} %param.13), kind=kLoop, calls=%fused_computation | loop fusion | flops 16777216 | bytes 50333696 | tf_op jit(solution)/shard_map/convert_element_type | solution.py:29
  35.8 3.9 pad_maximum_fusion
  39.6 5.1 all-to-all-done.3
  44.8 190.1 %all_to_all.51 = bf16[4,4,512,512]{3,2,1,0:T(8,128)(2,1)} all-to-all(bf16[4,4,512,512]{3,2,1,0:T(8,128)(2,1)} %pad_maximum_fusion), channel_id=1, replica_groups=mesh['grp'=2,'fs'=4,'tp'=4] {'fs'}, dimensions={0} | all-to-all | bytes 16777216 | tf_op jit(solution)/shard_map/all_to_all | solution.py:12
  234.8 5.6 all-to-all-start.1
  240.5 9.0 %convert_element_type.40 = bf16[16,512,512]{2,1,0:T(8,128)(2,1)} convert(f32[16,512,512]{2,1,0:T(8,128)} %param.15) | non-fusion elementwise | flops 4194304 | bytes 25165824 | tf_op jit(solution)/shard_map/convert_element_type | solution.py:30
  249.4 173.1 %all-to-all-done.1 = bf16[16,512,512]{2,1,0:T(8,128)(2,1)} async-done(((bf16[16,512,512]{2,1,0:T(8,128)(2,1)}), bf16[16,512,512]{2,1,0:T(8,128)(2,1)}, u32[]{:S(2)}, u32[]{:S(2)}) %all-to-all-start.1) | async-done | bytes 8388640 | tf_op jit(solution)/shard_map/all_to_all | solution.py:33
  422.5 5.7 all-to-all-start.2
  429.6 37.5 %all-gather.2.cloned.1.call-done = bf16[4,4,64,2048]{3,2,0,1:T(8,128)(2,1)} async-done(((bf16[4,4,64,512]{3,2,0,1:T(8,128)(2,1)}), bf16[4,4,64,2048]{3,2,0,1:T(8,128)(2,1)}) %all-gather.2.cloned.1.call-update) | async-done | bytes 4194320 | tf_op jit(solution)/shard_map/all_gather | solution.py:56
  467.1 3.1 multiply_reduce_fusion
  470.1 7.5 %copy.39 = bf16[4,4,512,512]{3,2,1,0:T(8,128)(2,1)} copy(bf16[4,4,512,512]{3,2,0,1:T(8,128)(2,1)} %bitcast.68) | data formatting | bytes 16777216 | tf_op jit(solution)/shard_map/reshape | solution.py:13
  477.7 7.5 %copy.40 = bf16[4,4,512,512]{3,2,0,1:T(8,128)(2,1)} copy(bf16[4,4,512,512]{3,2,1,0:T(8,128)(2,1)} %bitcast.6) | data formatting | bytes 16777216 | tf_op jit(solution)/shard_map/all_to_all | solution.py:33
  485.2 125.7 %all-to-all-done.2 = bf16[16,512,512]{2,1,0:T(8,128)(2,1)} async-done(((bf16[16,512,512]{2,1,0:T(8,128)(2,1)}), bf16[16,512,512]{2,1,0:T(8,128)(2,1)}, u32[]{:S(2)}, u32[]{:S(2)}) %all-to-all-start.2) | async-done | bytes 8388640 | tf_op jit(solution)/shard_map/all_to_all | solution.py:34
  610.8 7.7 %copy.41 = bf16[4,4,512,512]{3,2,0,1:T(8,128)(2,1)} copy(bf16[4,4,512,512]{3,2,1,0:T(8,128)(2,1)} %bitcast.9) | data formatting | bytes 16777216 | tf_op jit(solution)/shard_map/all_to_all | solution.py:34
  618.5 7.0 fusion.21
  625.6 14.2 %convert_bitcast_fusion = bf16[2048,4,4,64]{0,3,1,2:T(8,128)(2,1)} fusion(bf16[4,2048,512,1]{2,1,3,0:T(8,128)(2,1)} %bitcast.73, f32[4,4,64,512]{3,2,1,0:T(8,128)} %fusion.21, bf16[4,4,64,2048]{3,2,0,1:T(8,128)(2,1)} %all-gather.2.cloned.1.call-done, bf16[4,2048,512,1]{2,1,3,0:T(8,128)(2,1)} %bitcast.71, f32[4,4,64]{2,1,0:T(4,128)S(1)} %rsqrt_bitcast_fusion), kind=kOutput, calls=%fused_computation.4 | convolution fusion | flops 4301258752 | bytes 27267072 | tf_op jit(solution)/shard_map/edf,esxf->dsex/dot_general | solution.py:65
  639.7 43.7 %reduce-scatter.2.cloned.1.call-done = bf16[512,4,4,64]{0,3,1,2:T(8,128)(2,1)} async-done(((bf16[2048,4,4,64]{0,3,1,2:T(8,128)(2,1)}), bf16[512,4,4,64]{0,3,1,2:T(8,128)(2,1)}) %reduce-scatter.2.cloned.1.call-update) | async-done | bytes 1048592 | tf_op jit(solution)/shard_map/reduce_scatter | solution.py:64
  683.4 2.3 copy.47
  685.7 4.6 all-to-all-start.4
  690.3 25.5 %all-to-all-done.4 = bf16[512,4,4,64]{0,3,2,1:T(8,128)(2,1)S(1)} async-done(((bf16[512,4,4,64]{0,3,2,1:T(8,128)(2,1)}), bf16[512,4,4,64]{0,3,2,1:T(8,128)(2,1)S(1)}, u32[]{:S(2)}, u32[]{:S(2)}) %all-to-all-start.4) | async-done | bytes 1048608 | tf_op jit(solution)/shard_map/all_to_all | solution.py:72
  715.8 2.0 convolution_convert_fusion.1
  (31 shorter events, 5.9 us)
Async XLA Ops:
  7.2 4.0 copy-start
  12.7 32.1 %all-to-all-start.3 = ((bf16[4,4,64,512]{3,2,1,0:T(8,128)(2,1)}), bf16[4,4,64,512]{3,2,1,0:T(8,128)(2,1)S(1)}, u32[]{:S(2)}, u32[]{:S(2)}) async-start(bf16[4,4,64,512]{3,2,1,0:T(8,128)(2,1)} %bitcast.15), calls=%async_computation.3 | async-start | bytes 2097152 | tf_op jit(solution)/shard_map/all_to_all | solution.py:55
  234.8 187.7 %all-to-all-start.1 = ((bf16[16,512,512]{2,1,0:T(8,128)(2,1)}), bf16[16,512,512]{2,1,0:T(8,128)(2,1)}, u32[]{:S(2)}, u32[]{:S(2)}) async-start(bf16[16,512,512]{2,1,0:T(8,128)(2,1)} %get-tuple-element.10), calls=%async_computation.1 | async-start | bytes 16777216 | tf_op jit(solution)/shard_map/all_to_all | solution.py:33
  422.5 188.3 %all-to-all-start.2 = ((bf16[16,512,512]{2,1,0:T(8,128)(2,1)}), bf16[16,512,512]{2,1,0:T(8,128)(2,1)}, u32[]{:S(2)}, u32[]{:S(2)}) async-start(bf16[16,512,512]{2,1,0:T(8,128)(2,1)} %convert_element_type.40), calls=%async_computation.2 | async-start | bytes 16777216 | tf_op jit(solution)/shard_map/all_to_all | solution.py:34
  428.2 38.8 %all-gather.2.cloned.1.call-start = ((), (), s32[]{:S(2)}) async-start(), calls=%async_computation.6 | async-start | bytes 5242880 | tf_op jit(solution)/shard_map/all_gather | solution.py:56
  429.4 254.1 %reduce-scatter.2.cloned.1.call-start = ((), (), s32[]{:S(2)}) async-start(), calls=%async_computation.7 | async-start | bytes 5242880 | tf_op jit(solution)/shard_map/reduce_scatter | solution.py:64
  610.8 7.7 %copy-start.2 = (bf16[4,4,64,2048]{3,2,0,1:T(8,128)(2,1)S(1)}, bf16[4,4,64,2048]{3,2,0,1:T(8,128)(2,1)}, u32[]{:S(2)}) copy-start(bf16[4,4,64,2048]{3,2,0,1:T(8,128)(2,1)} %all-gather.2.cloned.1.call-done) | copy-start | bytes 12582916
  625.6 92.3 %copy-start.1 = (bf16[256,512]{1,0:T(8,128)(2,1)S(1)}, bf16[256,512]{1,0:T(8,128)(2,1)}, u32[]{:S(2)}) copy-start(bf16[256,512]{1,0:T(8,128)(2,1)} %param.8) | copy-start | bytes 786436
  639.7 50.6 %copy-start.3 = (f32[256]{0:T(256)S(1)}, f32[256]{0:T(256)}, u32[]{:S(2)}) copy-start(f32[256]{0:T(256)} %param.10) | copy-start | bytes 3076
  639.7 50.6 %copy-start.4 = (f32[256]{0:T(256)S(1)}, f32[256]{0:T(256)}, u32[]{:S(2)}) copy-start(f32[256]{0:T(256)} %param.11) | copy-start | bytes 3076
  685.7 30.1 %all-to-all-start.4 = ((bf16[512,4,4,64]{0,3,2,1:T(8,128)(2,1)}), bf16[512,4,4,64]{0,3,2,1:T(8,128)(2,1)S(1)}, u32[]{:S(2)}, u32[]{:S(2)}) async-start(bf16[512,4,4,64]{0,3,2,1:T(8,128)(2,1)} %copy.47), calls=%async_computation.5 | async-start | bytes 2097152 | tf_op jit(solution)/shard_map/all_to_all | solution.py:72
Sparse Core Ops, SparseCore 0:
  431.2 35.8 all-gather.1
  639.9 43.4 reduce-scatter.1
